TPU v7x, 32 devices: a whole 2x2x4 slice. The times are simulated.
32 devices in a mesh: sp: 8 (over z, x), tp: 4 (over y, core).
Axes of the slice: x: 2, y: 2, z: 4, core: 2. Of those that a mesh axis runs over, the one named last changes fastest.
Arguments:
- layer_input: bfloat16 [8, 4096, 2048], P(None, ('sp', 'tp')), may hold values from -6 to 6
- norm_gain: bfloat16 [2048], replicated, may hold values from 0.099609375 to 1.8984375
- key_weight: bfloat16 [2048, 1024], replicated, may hold values from -0.125 to 0.125
- value_weight: bfloat16 [2048, 1024], replicated, may hold values from -0.125 to 0.125
- new_query: bfloat16 [8, 1024], P('sp', 'tp'), may hold values from -12 to 12
- score_offset: float32 [8], replicated, may hold values from -10 to -3.5
Outputs:
- key_cache: bfloat16 [8, 4096, 1024], P('sp', None, 'tp')
- value_cache: bfloat16 [8, 4096, 1024], P('sp', None, 'tp')
- first_read: float32 [8, 1024], P('sp', 'tp')
All inputs are finite; a program needn't handle non-finite values.
Results may differ from a plain program's by a relative error of at most 0.0082.
Values may be sent and summed in bfloat16 or wider, within the bound.
A program may use at most 128 MiB of HBM per device.

v0:
```python
import jax
import jax.numpy as jnp
from jax import lax
from jax.sharding import PartitionSpec as P

norm_epsilon = 1e-06


def shards(layer_input, norm_gain, key_weight, value_weight, new_query, score_offset):
    seq_count, positions, model_width = layer_input.shape
    groups = lax.axis_size("tp")
    head_count = score_offset.shape[0]
    local_heads = head_count // groups
    head_dim = new_query.shape[1] // local_heads
    columns = local_heads * head_dim
    score_scale = head_dim ** (-0.5)
    wide = layer_input.astype(jnp.float32)
    normed = (
        wide
        * lax.rsqrt(jnp.mean(wide * wide, axis=-1, keepdims=True) + norm_epsilon)
        * norm_gain.astype(jnp.float32)
    ).astype(jnp.bfloat16)
    key_split = key_weight.reshape(model_width, groups, columns)
    value_split = value_weight.reshape(model_width, groups, columns)
    keys = jnp.einsum(
        "spd,dtc->stpc", normed, key_split, preferred_element_type=jnp.float32
    ).astype(jnp.bfloat16)
    values = jnp.einsum(
        "spd,dtc->stpc", normed, value_split, preferred_element_type=jnp.float32
    ).astype(jnp.bfloat16)
    stacked = jnp.stack((keys, values), axis=2)
    direct = stacked.reshape(seq_count * groups, 2, positions, columns)
    received = lax.all_to_all(direct, ("sp", "tp"), split_axis=0, concat_axis=2, tiled=True)
    arrived = received.reshape(2, -1, columns)
    key_cache = arrived[0][None]
    value_cache = arrived[1][None]
    own_keys = arrived[0].reshape(-1, local_heads, head_dim)
    own_values = arrived[1].reshape(-1, local_heads, head_dim)
    own_offsets = lax.dynamic_slice_in_dim(
        score_offset, lax.axis_index("tp") * local_heads, local_heads
    )
    query_own = new_query.reshape(local_heads, head_dim)
    scores = jnp.einsum("hd,phd->hp", query_own, own_keys, preferred_element_type=jnp.float32)
    scores = scores * score_scale + own_offsets[:, None]
    log_rest = jax.nn.log_sigmoid(-scores)
    later = lax.cumsum(log_rest, axis=1, reverse=True) - log_rest
    weights = jnp.exp(jax.nn.log_sigmoid(scores) + later).astype(jnp.bfloat16)
    reading = jnp.einsum("hp,phd->hd", weights, own_values, preferred_element_type=jnp.float32)
    first_read = reading * lax.rsqrt(
        jnp.mean(reading * reading, axis=-1, keepdims=True) + norm_epsilon
    )
    return (key_cache, value_cache, first_read.reshape(1, columns))


def solution(mesh):
    placed = (P(None, ("sp", "tp"), None), P(), P(), P(), P("sp", "tp"), P())
    return jax.shard_map(
        shards,
        mesh=mesh,
        in_specs=placed,
        out_specs=(P("sp", None, "tp"), P("sp", None, "tp"), P("sp", "tp")),
        check_vma=False,
    )
```

profile of v0, /device:TPU:0, one launch (start us, length us, event | category | flops | bytes accessed | tf_op | source)
XLA Modules:
  0.0 139.0 jit_solution(2495934026409444317)
XLA Ops:
  0.6 0.0 copy-start
  0.6 0.0 copy-start.2
  0.7 3.2 %fusion = f32[8,128]{1,0:T(8,128)S(1)} fusion(bf16[8,128,2048]{2,1,0:T(8,128)(2,1)} %param.6), kind=kLoop, calls=%fused_computation.2 | loop fusion | flops 6290432 | bytes 4198400 | tf_op jit(solution)/shard_map/reduce_sum | solution.py:20
  3.9 0.2 copy-done.2
  4.1 7.2 %fusion.17 = bf16[8,128,4,256]{3,1,2,0:T(8,128)(2,1)S(1)} fusion(bf16[256,4,8,256]{3,2,1,0:T(8,128)(2,1)} %bitcast.94, bf16[8,128,2048]{2,1,0:T(8,128)(2,1)S(1)} %copy-done.2, f32[2048]{0:T(1024)S(1)} %convert_element_type.25, f32[8,128]{1,0:T(8,128)S(1)} %add_rsqrt_fusion), kind=kOutput, calls=%fused_computation.18 | convolution fusion | flops 4304404480 | bytes 10498048 | tf_op jit(solution)/shard_map/spd,dtc->stpc/dot_general | solution.py:28
  11.3 4.8 %fusion.14 = bf16[8,128,4,256]{3,1,2,0:T(8,128)(2,1)S(1)} fusion(bf16[256,4,8,256]{3,2,1,0:T(8,128)(2,1)S(1)} %bitcast.95, bf16[8,128,2048]{2,1,0:T(8,128)(2,1)S(1)} %copy-done.2, f32[2048]{0:T(1024)S(1)} %convert_element_type.25, f32[8,128]{1,0:T(8,128)S(1)} %add_rsqrt_fusion), kind=kOutput, calls=%fused_computation.17 | convolution fusion | flops 4304404480 | bytes 10498048 | tf_op jit(solution)/shard_map/spd,dtc->stpc/dot_general | solution.py:25
  16.2 2.3 %pad_maximum_fusion = bf16[32,2,128,256]{3,2,1,0:T(8,128)(2,1)} fusion(bf16[32,1,128,256]{3,2,1,0:T(8,128)(2,1)S(1)} %bitcast.88, bf16[32,1,128,256]{3,2,1,0:T(8,128)(2,1)S(1)} %bitcast.89), kind=kLoop, calls=%fused_computation.12 | loop fusion | flops 2097152 | bytes 8388608 | tf_op jit(solution)/shard_map/stack | solution.py:31
  18.5 7.5 %all-to-all-start = ((bf16[32,2,128,256]{3,2,1,0:T(8,128)(2,1)}), bf16[32,2,128,256]{3,2,1,0:T(8,128)(2,1)}, u32[]{:S(2)}, u32[]{:S(2)}) async-start(bf16[32,2,128,256]{3,2,1,0:T(8,128)(2,1)} %pad_maximum_fusion), calls=%async_computation | async-start | bytes 8388608 | tf_op jit(solution)/shard_map/all_to_all | solution.py:33
  26.0 0.1 dynamic_slice.3
  26.1 94.1 %all-to-all-done = bf16[32,2,128,256]{3,2,1,0:T(8,128)(2,1)} async-done(((bf16[32,2,128,256]{3,2,1,0:T(8,128)(2,1)}), bf16[32,2,128,256]{3,2,1,0:T(8,128)(2,1)}, u32[]{:S(2)}, u32[]{:S(2)}) %all-to-all-start) | async-done | bytes 4194336 | tf_op jit(solution)/shard_map/all_to_all | solution.py:33
  120.2 3.9 %fusion.30 = (bf16[1,1,32,128,256]{4,3,1,2,0:T(8,128)(2,1)S(1)}, bf16[1,1,32,128,256]{4,3,1,2,0:T(8,128)(2,1)}) fusion(bf16[1,2,32,128,256]{4,3,1,2,0:T(8,128)(2,1)} %bitcast.12), kind=kLoop, calls=%fused_computation.40 | loop fusion | bytes 8388608 | tf_op jit(solution)/shard_map/slice | solution.py:36
  124.2 4.3 %reshape_squeeze.6 = bf16[4096,2,128]{2,1,0:T(2,128)(2,1)} reshape(bf16[1,1,32,128,256]{4,3,1,2,0:T(8,128)(2,1)} %get-tuple-element.4) | data formatting | bytes 4194304 | tf_op jit(solution)/shard_map/reshape;squeeze | solution.py:37
  128.5 2.2 %fusion.12 = f32[2,1,4096]{2,1,0:T(1,128)S(1)} fusion(bf16[4096,2,128]{2,1,0:T(2,128)(2,1)} %reshape_squeeze.6, bf16[1,256]{1,0:T(2,128)(2,1)S(1)} %copy-done), kind=kOutput, calls=%fused_computation.15 | convolution fusion | flops 2097152 | bytes 2130432 | tf_op jit(solution)/shard_map/hd,phd->hp/dot_general | solution.py:43
  130.7 0.2 fusion.29
  130.9 2.5 %reduce-window.6 = f32[2,32,128]{2,1,0:T(8,128)S(1)} reduce-window(f32[2,32,128]{2,1,0:T(8,128)S(1)} %bitcast.90, f32[]{:T(128)} %constant.9.clone.1), window={size=1x1x128 pad=0_0x0_0x0_127}, to_apply=%region_1.2 | reduce-window | flops 1040384 | bytes 65540 | tf_op jit(solution)/shard_map/reduce-window
  133.4 0.1 slice_reduce_fusion
  133.5 0.3 reduce-window.9
  133.8 0.1 slice.25
  133.8 0.1 add_bitcast_fusion
  133.9 0.3 fusion.27
  134.2 2.1 %reshape_squeeze.7 = bf16[4096,2,128]{2,1,0:T(2,128)(2,1)} reshape(bf16[1,1,32,128,256]{4,3,1,2,0:T(8,128)(2,1)S(1)} %get-tuple-element.3) | data formatting | bytes 4194304 | tf_op jit(solution)/shard_map/reshape;squeeze | solution.py:38
  136.3 2.0 %fusion.10 = f32[2,1,128]{2,1,0:T(1,128)S(1)} fusion(bf16[4096,2,128]{2,1,0:T(2,128)(2,1)} %reshape_squeeze.7, bf16[2,4096,1]{1,0,2:T(2,128)(2,1)S(1)} %fusion.27), kind=kOutput, calls=%fused_computation.13 | convolution fusion | flops 2097152 | bytes 2114560 | tf_op jit(solution)/shard_map/hp,phd->hd/dot_general | solution.py:48
  138.3 0.1 multiply_reduce_fusion
  138.4 0.6 broadcast_multiply_fusion
  (13 shorter events, 0.0 us)
Async XLA Ops:
  0.6 127.9 %copy-start = (bf16[1,256]{1,0:T(2,128)(2,1)S(1)}, bf16[1,256]{1,0:T(2,128)(2,1)}, u32[]{:S(2)}) copy-start(bf16[1,256]{1,0:T(2,128)(2,1)} %param.10) | copy-start | bytes 1540
  0.6 3.5 %copy-start.2 = (bf16[8,128,2048]{2,1,0:T(8,128)(2,1)S(1)}, bf16[8,128,2048]{2,1,0:T(8,128)(2,1)}, u32[]{:S(2)}) copy-start(bf16[8,128,2048]{2,1,0:T(8,128)(2,1)} %param.6) | copy-start | bytes 12582916
  0.7 3.3 %copy-start.3 = (bf16[2048]{0:T(1024)(128)(2,1)S(1)}, bf16[2048]{0:T(1024)(128)(2,1)}, u32[]{:S(2)}) copy-start(bf16[2048]{0:T(1024)(128)(2,1)} %param.7) | copy-start | bytes 12292
  4.1 7.2 %copy-start.4 = (bf16[2048,1024]{1,0:T(8,128)(2,1)S(1)}, bf16[2048,1024]{1,0:T(8,128)(2,1)}, u32[]{:S(2)}) copy-start(bf16[2048,1024]{1,0:T(8,128)(2,1)} %param.8) | copy-start | bytes 12582916
  18.5 7.5 %copy-start.5 = (f32[8]{0:T(128)S(1)}, f32[8]{0:T(128)}, u32[]{:S(2)}) copy-start(f32[8]{0:T(128)} %param.11) | copy-start | bytes 100
  18.5 101.7 %all-to-all-start = ((bf16[32,2,128,256]{3,2,1,0:T(8,128)(2,1)}), bf16[32,2,128,256]{3,2,1,0:T(8,128)(2,1)}, u32[]{:S(2)}, u32[]{:S(2)}) async-start(bf16[32,2,128,256]{3,2,1,0:T(8,128)(2,1)} %pad_maximum_fusion), calls=%async_computation | async-start | bytes 8388608 | tf_op jit(solution)/shard_map/all_to_all | solution.py:33
  124.2 12.1 %copy-start.1 = (bf16[1,1,32,128,256]{4,3,1,2,0:T(8,128)(2,1)}, bf16[1,1,32,128,256]{4,3,1,2,0:T(8,128)(2,1)S(1)}, u32[]{:S(2)}) copy-start(bf16[1,1,32,128,256]{4,3,1,2,0:T(8,128)(2,1)S(1)} %get-tuple-element.3) | copy-start | bytes 6291460
where the time goes:
time: 139 us
  waiting for transfers between devices  94.1 us (68%)
  matrix products  16.2 us (12%)
  local copies, waits for them, and re-layouts  10.8 us (8%)
  other arithmetic  9.61 us (7%)
  starting transfers between devices  7.46 us (5%)
    all_to_all x1, waiting for transfers between devices, shards(): lax.all_to_all(direct, ('sp', 'tp'), split_axis=0, concat_axis=2, tiled=T...  94.1 us
    all_to_all x1, starting transfers between devices, shards(): lax.all_to_all(direct, ('sp', 'tp'), split_axis=0, concat_axis=2, tiled=T...  7.46 us
    dot_general x1, matrix products, shards(): jnp.einsum('spd,dtc->stpc', normed, value_split, preferred_element_type=j...  7.19 us
    dot_general x1, matrix products, shards(): jnp.einsum('spd,dtc->stpc', normed, key_split, preferred_element_type=jnp...  4.84 us
    another operation x1, local copies, waits for them, and re-layouts, shards(): own_keys = arrived[0].reshape(-1, local_heads, head_dim)  4.32 us
    slice x1, local copies, waits for them, and re-layouts, shards(): value_cache = arrived[1][None]  3.93 us
    reduce_sum x1, other arithmetic, shards(): jnp.mean(wide * wide, axis=-1, keepdims=True) + norm_epsilon  3.23 us
  transfers between devices with their start and end apart: 1, of which 1 were waited for; matrix products, arithmetic and copies ran while one was open for 0% of the time, Pallas kernels for 0%

commit v1 on v0

v1 whole, which is shorter than its diff:
```python
import functools

import jax
import jax.numpy as jnp
from jax import lax
from jax.experimental import pallas as pl
from jax.experimental.pallas import tpu as pltpu
from jax.sharding import PartitionSpec as P

norm_epsilon = 1e-06
MESH = pl.DeviceIdType.MESH
NORM_ROWS = 16


def exchange_kernel(
    seqs,
    groups,
    local_heads,
    x_hbm,
    gain_ref,
    key_w_hbm,
    value_w_hbm,
    query_ref,
    offset_ref,
    key_out,
    value_out,
    read_ref,
    x_buf,
    normed,
    key_w,
    value_w,
    outgoing,
    arrived,
    group_read,
    group_rest,
    x_sem,
    w_sem,
    send_sem,
    recv_sem,
    out_sem,
):
    positions = x_buf.shape[1]
    width = x_buf.shape[2]
    columns = query_ref.shape[1]
    head_dim = columns // local_heads
    span = groups * positions
    pad = group_read.shape[1]
    my_seq = lax.axis_index("sp")
    my_group = lax.axis_index("tp")
    me = my_seq * groups + my_group
    upper = (my_seq >= seqs // 2).astype(jnp.int32)
    pair = (my_seq // 2) * 2

    def seq_at(step):
        ahead = lax.rem(pair + 2 + step, seqs)
        behind = lax.rem(pair - 1 - step + 2 * seqs, seqs)
        return upper * behind + (1 - upper) * ahead

    def x_copy(step):
        seq = seq_at(step)
        return pltpu.make_async_copy(x_hbm.at[seq], x_buf.at[step], x_sem.at[step])

    def w_copy(index):
        cols = pl.ds(pl.multiple_of(index * columns, columns), columns)
        return (
            pltpu.make_async_copy(key_w_hbm.at[:, cols], key_w.at[index], w_sem.at[0, index]),
            pltpu.make_async_copy(value_w_hbm.at[:, cols], value_w.at[index], w_sem.at[1, index]),
        )

    def target(turn):
        return lax.rem(my_group + 1 + turn, groups)

    x_copy(0).start()
    for turn in range(groups):
        for copy in w_copy(target(turn)):
            copy.start()
        if turn == 0 and seqs > 1:
            x_copy(1).start()

    @pl.loop(2, seqs)
    def _(step):
        x_copy(step).start()

    barrier = pltpu.get_barrier_semaphore()

    @pl.loop(0, seqs * groups)
    def _(device):
        @pl.when(device != me)
        def _():
            pl.semaphore_signal(
                barrier,
                inc=1,
                device_id=(device // groups, lax.rem(device, groups)),
                device_id_type=MESH,
            )

    def block_rows(device):
        return pl.ds(pl.multiple_of(device * positions, positions), positions)

    def remote(seq, group):
        device = seq * groups + group
        return pltpu.make_async_remote_copy(
            src_ref=outgoing.at[seq, group],
            dst_ref=arrived.at[block_rows(me)],
            send_sem=send_sem.at[device],
            recv_sem=recv_sem.at[me],
            device_id=(seq, group),
            device_id_type=MESH,
        )

    def own():
        return pltpu.make_async_copy(
            outgoing.at[my_seq, my_group], arrived.at[block_rows(me)], recv_sem.at[me]
        )

    def launch(seq, group):
        mine = seq * groups + group == me

        @pl.when(mine)
        def _():
            own().start()

        @pl.when(jnp.logical_not(mine))
        def _():
            remote(seq, group).start()

    def norm(step):
        x_copy(step).wait()

        @pl.loop(0, positions // NORM_ROWS)
        def _(chunk):
            rows = pl.ds(pl.multiple_of(chunk * NORM_ROWS, NORM_ROWS), NORM_ROWS)
            wide = x_buf[step, rows, :].astype(jnp.float32)
            scale = lax.rsqrt(jnp.sum(wide * wide, axis=-1, keepdims=True) / width + norm_epsilon)
            normed[rows, :] = (wide * scale * gain_ref[...].astype(jnp.float32)).astype(jnp.bfloat16)

    def project(step, turn):
        seq = seq_at(step)
        group = target(turn)
        outgoing[seq, group, :, :columns] = jnp.dot(
            normed[...], key_w[group], preferred_element_type=jnp.float32
        ).astype(jnp.bfloat16)
        outgoing[seq, group, :, columns:] = jnp.dot(
            normed[...], value_w[group], preferred_element_type=jnp.float32
        ).astype(jnp.bfloat16)

    norm(0)

    @pl.loop(0, groups)
    def _(turn):
        for copy in w_copy(target(turn)):
            copy.wait()
        project(0, turn)

        @pl.when(turn == 0)
        def _():
            pl.semaphore_wait(barrier, seqs * groups - 1)

        @pl.when(turn > 0)
        def _():
            launch(seq_at(0), target(turn - 1))

    @pl.loop(1, seqs)
    def _(step):
        norm(step)
        launch(seq_at(step - 1), target(groups - 1))

        @pl.loop(0, groups)
        def _(turn):
            project(step, turn)

            @pl.when(turn > 0)
            def _():
                launch(seq_at(step), target(turn - 1))

    row = lax.broadcasted_iota(jnp.int32, (pad, columns), 0)
    col = lax.broadcasted_iota(jnp.int32, (pad, columns), 1)
    query = jnp.where(
        row == col // head_dim,
        jnp.broadcast_to(query_ref[...].astype(jnp.float32), (pad, columns)),
        0.0,
    ).astype(jnp.bfloat16)
    launch(seq_at(seqs - 1), target(groups - 1))

    score_row = lax.broadcasted_iota(jnp.int32, (pad, span), 0)
    score_col = lax.broadcasted_iota(jnp.int32, (pad, span), 1)
    offsets = jnp.zeros((pad, span), jnp.float32)
    for head in range(local_heads):
        offsets = jnp.where(score_row == head, offset_ref[my_group * local_heads + head], offsets)

    def out_copies(seq):
        rows = pl.ds(pl.multiple_of(seq * span, span), span)
        return (
            pltpu.make_async_copy(
                arrived.at[rows, pl.ds(0, columns)], key_out.at[rows], out_sem.at[0, seq]
            ),
            pltpu.make_async_copy(
                arrived.at[rows, pl.ds(columns, columns)], value_out.at[rows], out_sem.at[1, seq]
            ),
        )

    @pl.loop(0, seqs)
    def _(turn):
        seq = upper * (seqs - 1 - turn) + (1 - upper) * turn

        @pl.loop(0, groups)
        def _(group):
            device = seq * groups + group
            pltpu.make_async_copy(
                outgoing.at[seq, group], arrived.at[block_rows(device)], recv_sem.at[device]
            ).wait()

        for copy in out_copies(seq):
            copy.start()
        rows = pl.ds(pl.multiple_of(seq * span, span), span)
        scores = lax.dot_general(
            query,
            arrived[rows, :columns],
            (((1,), (1,)), ((), ())),
            preferred_element_type=jnp.float32,
        )
        scores = scores * head_dim ** (-0.5) + offsets
        soft = jnp.log1p(jnp.exp(-jnp.abs(scores)))
        rest = -jnp.maximum(scores, 0.0) - soft
        total = rest
        shift = 1
        while shift < span:
            total = total + jnp.where(
                score_col < span - shift, pltpu.roll(total, span - shift, 1), 0.0
            )
            shift *= 2
        later = total - rest
        weights = jnp.exp(jnp.minimum(scores, 0.0) - soft + later).astype(jnp.bfloat16)
        group_read[seq] = jnp.dot(
            weights, arrived[rows, columns:], preferred_element_type=jnp.float32
        )
        group_rest[seq] = jnp.broadcast_to(total[:, :1], (pad, columns))

    reading = jnp.zeros((pad, columns), jnp.float32)
    after = jnp.zeros((pad, columns), jnp.float32)
    for seq in reversed(range(seqs)):
        reading = reading + jnp.exp(after) * group_read[seq]
        after = after + group_rest[seq]
    for head in range(local_heads):
        own_cols = slice(head * head_dim, (head + 1) * head_dim)
        part = reading[head : head + 1, own_cols]
        read_ref[:, own_cols] = part * lax.rsqrt(
            jnp.mean(part * part, axis=-1, keepdims=True) + norm_epsilon
        )

    @pl.loop(0, seqs * groups)
    def _(device):
        @pl.when(device != me)
        def _():
            remote(device // groups, lax.rem(device, groups)).wait_send()

    @pl.loop(0, seqs)
    def _(seq):
        for copy in out_copies(seq):
            copy.wait()


def shards(seqs, groups, layer_input, norm_gain, key_weight, value_weight, new_query, score_offset):
    seq_count, positions, width = layer_input.shape
    columns = new_query.shape[1]
    local_heads = score_offset.shape[0] // groups
    pad = -(-local_heads // 8) * 8
    length = seqs * groups * positions
    any_space = pl.BlockSpec(memory_space=pl.ANY)
    vmem = pl.BlockSpec(memory_space=pltpu.VMEM)
    keys, values, read = pl.pallas_call(
        functools.partial(exchange_kernel, seqs, groups, local_heads),
        out_shape=(
            jax.ShapeDtypeStruct((length, columns), jnp.bfloat16),
            jax.ShapeDtypeStruct((length, columns), jnp.bfloat16),
            jax.ShapeDtypeStruct((1, columns), jnp.float32),
        ),
        in_specs=[
            any_space,
            vmem,
            any_space,
            any_space,
            vmem,
            pl.BlockSpec(memory_space=pltpu.SMEM),
        ],
        out_specs=(any_space, any_space, vmem),
        scratch_shapes=[
            pltpu.VMEM((seq_count, positions, width), jnp.bfloat16),
            pltpu.VMEM((positions, width), jnp.bfloat16),
            pltpu.VMEM((groups, width, columns), jnp.bfloat16),
            pltpu.VMEM((groups, width, columns), jnp.bfloat16),
            pltpu.VMEM((seqs, groups, positions, 2 * columns), jnp.bfloat16),
            pltpu.VMEM((length, 2 * columns), jnp.bfloat16),
            pltpu.VMEM((seqs, pad, columns), jnp.float32),
            pltpu.VMEM((seqs, pad, columns), jnp.float32),
            pltpu.SemaphoreType.DMA((seq_count,)),
            pltpu.SemaphoreType.DMA((2, groups)),
            pltpu.SemaphoreType.DMA((seqs * groups,)),
            pltpu.SemaphoreType.DMA((seqs * groups,)),
            pltpu.SemaphoreType.DMA((2, seqs)),
        ],
        compiler_params=pltpu.CompilerParams(
            collective_id=0, has_side_effects=True, vmem_limit_bytes=67043328
        ),
    )(layer_input, norm_gain.reshape(1, width), key_weight, value_weight, new_query, score_offset)
    return (keys[None], values[None], read)


def solution(mesh):
    seqs = mesh.shape["sp"]
    groups = mesh.shape["tp"]
    placed = (P(None, ("sp", "tp"), None), P(), P(), P(), P("sp", "tp"), P())
    return jax.shard_map(
        functools.partial(shards, seqs, groups),
        mesh=mesh,
        in_specs=placed,
        out_specs=(P("sp", None, "tp"), P("sp", None, "tp"), P("sp", "tp")),
        check_vma=False,
    )
```

time: 139 us -> 117 us (0.84)
  Pallas kernels: 0 us -> 110 us
  waiting for transfers between devices: 94.1 us -> 0 us
  matrix products: 16.2 us -> 0 us
  other arithmetic: 9.61 us -> 0 us
  starting transfers between devices: 7.46 us -> 0 us
  local copies, waits for them, and re-layouts: 10.8 us -> 6.37 us
    pallas_call x0 -> x1, Pallas kernels: none -> 110 us  [shards(): pl.pallas_call(functools.partial(exchange_kernel, seqs, groups, local_hea...]
    all_to_all x1 -> x0, waiting for transfers between devices: 94.1 us -> none  [shards(): lax.all_to_all(direct, ('sp', 'tp'), split_axis=0, concat_axis=2, tiled=T...]
    dot_general x4 -> x0, matrix products: 16.2 us -> none  [the longest x1 7.19 us: shards(): jnp.einsum('spd,dtc->stpc', normed, value_split, preferred_element_type=j...]
    all_to_all x1 -> x0, starting transfers between devices: 7.46 us -> none  [shards(): lax.all_to_all(direct, ('sp', 'tp'), split_axis=0, concat_axis=2, tiled=T...]
    another operation x3 -> x0, local copies, waits for them, and re-layouts: 6.49 us -> none  [the longest x1 4.32 us: shards(): own_keys = arrived[0].reshape(-1, local_heads, head_dim)]
    another operation x3 -> x0, other arithmetic: 5.09 us -> none
    unnamed x13 -> x7, local copies, waits for them, and re-layouts: 0.22 us -> 5.08 us
    slice x2 -> x0, local copies, waits for them, and re-layouts: 4.02 us -> none  [the longest x1 3.93 us: shards(): value_cache = arrived[1][None]]
  transfers between devices with their start and end apart: 1 -> 0, of which waited for: 1 -> 0; matrix products, arithmetic and copies ran while one was open for 0% -> 0% of each run, Pallas kernels for 0% -> 0%
where the time goes in v1:
time: 117 us
  Pallas kernels  110 us (94%)
  local copies, waits for them, and re-layouts  6.37 us (5%)
    pallas_call x1, Pallas kernels, shards(): pl.pallas_call(functools.partial(exchange_kernel, seqs, groups, local_hea...  110 us
    unnamed x7, local copies, waits for them, and re-layouts  5.08 us

profile of v1, /device:TPU:0, one launch (start us, length us, event | category | flops | bytes accessed | tf_op | source)
XLA Modules:
  0.0 117.0 jit_solution(14603208057258381610)
XLA Ops:
  0.6 1.3 %reshape.9.gain_ref = bf16[1,2048]{1,0:T(2,128)(2,1)} reshape(bf16[2048]{0:T(1024)(128)(2,1)} %param.7) | data formatting | bytes 8192 | tf_op jit(solution)/shard_map/reshape | solution.py:305
  1.9 110.0 %shard_map.85 = (bf16[4096,256]{1,0:T(8,128)(2,1)}, bf16[4096,256]{1,0:T(8,128)(2,1)}, f32[1,256]{1,0:T(1,128)}) custom-call(bf16[8,128,2048]{2,1,0:T(8,128)(2,1)} %x_hbm.1, bf16[1,2048]{1,0:T(2,128)(2,1)} %reshape.9.gain_ref, bf16[2048,1024]{1,0:T(8,128)(2,1)} %key_w_hbm.1, bf16[2048,1024]{1,0:T(8,128)(2,1)} %value_w_hbm.1, bf16[1,256]{1,0:T(2,128)(2,1)} %query_ref.1, ...), custom_call_target="tpu_custom_call" | custom-call | tf_op jit(solution)/shard_map/pallas_call | solution.py:271
  111.9 0.0 copy-start
  111.9 3.2 %copy.12 = bf16[1,4096,256]{2,1,0:T(8,128)(2,1)} copy(bf16[1,4096,256]{2,1,0:T(8,128)(2,1)} %bitcast.3) | data formatting | bytes 4194304
  115.1 0.0 copy-done
  115.1 0.0 copy-start.1
  115.1 1.3 %copy.13 = bf16[1,4096,256]{2,1,0:T(8,128)(2,1)} copy(bf16[1,4096,256]{2,1,0:T(8,128)(2,1)S(1)} %bitcast.2) | data formatting | bytes 4194304
  116.4 0.0 copy-done.1
  116.4 0.6 copy.14
Async XLA Ops:
  111.9 3.2 %copy-start = (bf16[4096,256]{1,0:T(8,128)(2,1)S(1)}, bf16[4096,256]{1,0:T(8,128)(2,1)}, u32[]{:S(2)}) copy-start(bf16[4096,256]{1,0:T(8,128)(2,1)} %get-tuple-element.7) | copy-start | bytes 6291460
  115.1 1.3 %copy-start.1 = (f32[1,256]{1,0:T(1,128)S(1)}, f32[1,256]{1,0:T(1,128)}, u32[]{:S(2)}) copy-start(f32[1,256]{1,0:T(1,128)} %get-tuple-element.14) | copy-start | bytes 3076

commit v2 on v1

--- a/solution.py
+++ b/solution.py
@@ -51,10 +51,16 @@
     upper = (my_seq >= seqs // 2).astype(jnp.int32)
     pair = (my_seq // 2) * 2
 
+    quad = 4 if seqs % 4 == 0 else 1
+
     def seq_at(step):
-        ahead = lax.rem(pair + 2 + step, seqs)
-        behind = lax.rem(pair - 1 - step + 2 * seqs, seqs)
-        return upper * behind + (1 - upper) * ahead
+        if quad == 1:
+            return lax.rem(my_seq + 1 + step, seqs)
+        jump = 2 * (step // 4) + lax.rem(step, 2)
+        side = lax.rem(my_seq + lax.rem(step // 2, 2), 2)
+        ahead = lax.rem(pair + 2 + 2 * jump, seqs)
+        behind = lax.rem(pair - 2 - 2 * jump + 2 * seqs, seqs)
+        return upper * behind + (1 - upper) * ahead + side
 
     def x_copy(step):
         seq = seq_at(step)
@@ -68,14 +74,17 @@
         )
 
     def target(turn):
-        return lax.rem(my_group + 1 + turn, groups)
-
-    x_copy(0).start()
+        turn = lax.rem(turn + my_seq // 2, groups)
+        if groups % 2 == 0:
+            turn = turn // 2 + lax.rem(turn, 2) * (groups // 2)
+        return lax.rem(my_group + turn, groups)
+
+    x_copy(jnp.int32(0)).start()
     for turn in range(groups):
-        for copy in w_copy(target(turn)):
+        for copy in w_copy(target(jnp.int32(turn))):
             copy.start()
         if turn == 0 and seqs > 1:
-            x_copy(1).start()
+            x_copy(jnp.int32(1)).start()
 
     @pl.loop(2, seqs)
     def _(step):
@@ -126,52 +135,58 @@
 
     def norm(step):
         x_copy(step).wait()
+        slot = lax.rem(step, quad)
 
         @pl.loop(0, positions // NORM_ROWS)
         def _(chunk):
             rows = pl.ds(pl.multiple_of(chunk * NORM_ROWS, NORM_ROWS), NORM_ROWS)
             wide = x_buf[step, rows, :].astype(jnp.float32)
             scale = lax.rsqrt(jnp.sum(wide * wide, axis=-1, keepdims=True) / width + norm_epsilon)
-            normed[rows, :] = (wide * scale * gain_ref[...].astype(jnp.float32)).astype(jnp.bfloat16)
+            gain = gain_ref[...].astype(jnp.float32).reshape(1, width)
+            normed[slot, rows, :] = (wide * scale * gain).astype(jnp.bfloat16)
 
     def project(step, turn):
         seq = seq_at(step)
         group = target(turn)
+        slot = lax.rem(step, quad)
         outgoing[seq, group, :, :columns] = jnp.dot(
-            normed[...], key_w[group], preferred_element_type=jnp.float32
+            normed[slot], key_w[group], preferred_element_type=jnp.float32
         ).astype(jnp.bfloat16)
         outgoing[seq, group, :, columns:] = jnp.dot(
-            normed[...], value_w[group], preferred_element_type=jnp.float32
+            normed[slot], value_w[group], preferred_element_type=jnp.float32
         ).astype(jnp.bfloat16)
 
-    norm(0)
-
-    @pl.loop(0, groups)
-    def _(turn):
-        for copy in w_copy(target(turn)):
-            copy.wait()
-        project(0, turn)
+    def place(index):
+        phase = index // (quad * groups)
+        within = lax.rem(index, quad * groups)
+        return phase * quad + lax.rem(within, quad), within // quad
+
+    def launch_at(index):
+        step, turn = place(index)
+        launch(seq_at(step), target(turn))
+
+    @pl.loop(0, seqs * groups)
+    def _(index):
+        step, turn = place(index)
 
         @pl.when(turn == 0)
         def _():
+            norm(step)
+
+        @pl.when(step == 0)
+        def _():
+            for copy in w_copy(target(turn)):
+                copy.wait()
+
+        project(step, turn)
+
+        @pl.when(index == 0)
+        def _():
             pl.semaphore_wait(barrier, seqs * groups - 1)
 
-        @pl.when(turn > 0)
-        def _():
-            launch(seq_at(0), target(turn - 1))
-
-    @pl.loop(1, seqs)
-    def _(step):
-        norm(step)
-        launch(seq_at(step - 1), target(groups - 1))
-
-        @pl.loop(0, groups)
-        def _(turn):
-            project(step, turn)
-
-            @pl.when(turn > 0)
-            def _():
-                launch(seq_at(step), target(turn - 1))
+        @pl.when(index > 0)
+        def _():
+            launch_at(index - 1)
 
     row = lax.broadcasted_iota(jnp.int32, (pad, columns), 0)
     col = lax.broadcasted_iota(jnp.int32, (pad, columns), 1)
@@ -180,7 +195,7 @@
         jnp.broadcast_to(query_ref[...].astype(jnp.float32), (pad, columns)),
         0.0,
     ).astype(jnp.bfloat16)
-    launch(seq_at(seqs - 1), target(groups - 1))
+    launch_at(jnp.int32(seqs * groups - 1))
 
     score_row = lax.broadcasted_iota(jnp.int32, (pad, span), 0)
     score_col = lax.broadcasted_iota(jnp.int32, (pad, span), 1)
@@ -271,8 +286,8 @@
     keys, values, read = pl.pallas_call(
         functools.partial(exchange_kernel, seqs, groups, local_heads),
         out_shape=(
-            jax.ShapeDtypeStruct((length, columns), jnp.bfloat16),
-            jax.ShapeDtypeStruct((length, columns), jnp.bfloat16),
+            pltpu.VMEM((length, columns), jnp.bfloat16),
+            pltpu.VMEM((length, columns), jnp.bfloat16),
             jax.ShapeDtypeStruct((1, columns), jnp.float32),
         ),
         in_specs=[
@@ -283,10 +298,10 @@
             vmem,
             pl.BlockSpec(memory_space=pltpu.SMEM),
         ],
-        out_specs=(any_space, any_space, vmem),
+        out_specs=(vmem, vmem, vmem),
         scratch_shapes=[
             pltpu.VMEM((seq_count, positions, width), jnp.bfloat16),
-            pltpu.VMEM((positions, width), jnp.bfloat16),
+            pltpu.VMEM((4 if seqs % 4 == 0 else 1, positions, width), jnp.bfloat16),
             pltpu.VMEM((groups, width, columns), jnp.bfloat16),
             pltpu.VMEM((groups, width, columns), jnp.bfloat16),
             pltpu.VMEM((seqs, groups, positions, 2 * columns), jnp.bfloat16),
@@ -300,9 +315,9 @@
             pltpu.SemaphoreType.DMA((2, seqs)),
         ],
         compiler_params=pltpu.CompilerParams(
-            collective_id=0, has_side_effects=True, vmem_limit_bytes=67043328
+            collective_id=0, has_side_effects=True, vmem_limit_bytes=50000000
         ),
-    )(layer_input, norm_gain.reshape(1, width), key_weight, value_weight, new_query, score_offset)
+    )(layer_input, norm_gain, key_weight, value_weight, new_query, score_offset)
     return (keys[None], values[None], read)
 
 

time: 117 us -> 113 us (0.966)
  Pallas kernels: 110 us -> 107 us
    pallas_call x1, Pallas kernels: 110 us -> 107 us  [shards(): pl.pallas_call(functools.partial(exchange_kernel, seqs, groups, local_hea...]
    reshape x1 -> x0, local copies, waits for them, and re-layouts: 1.29 us -> none  [shards(): norm_gain.reshape(1, width)]
    unnamed x7 -> x9, local copies, waits for them, and re-layouts: 5.08 us -> 5.21 us
where the time goes in v2:
time: 113 us
  Pallas kernels  107 us (95%)
  local copies, waits for them, and re-layouts  5.21 us (5%)
    pallas_call x1, Pallas kernels, shards(): pl.pallas_call(functools.partial(exchange_kernel, seqs, groups, local_hea...  107 us
    unnamed x9, local copies, waits for them, and re-layouts  5.21 us

profile of v2, /device:TPU:0, one launch (start us, length us, event | category | flops | bytes accessed | tf_op | source)
XLA Modules:
  0.0 112.8 jit_solution(5782767688503112973)
XLA Ops:
  0.6 0.0 copy-start
  0.6 0.7 copy-done
  1.3 0.0 copy-start.1
  1.3 0.7 copy-done.1
  2.0 0.0 copy-start.2
  2.0 0.7 copy-done.2
  2.7 106.9 %shard_map.85 = (bf16[4096,256]{1,0:T(8,128)(2,1)S(1)}, bf16[4096,256]{1,0:T(8,128)(2,1)S(1)}, f32[1,256]{1,0:T(1,128)S(1)}) custom-call(bf16[8,128,2048]{2,1,0:T(8,128)(2,1)} %x_hbm.1, bf16[2048]{0:T(1024)(128)(2,1)S(1)} %copy-done, bf16[2048,1024]{1,0:T(8,128)(2,1)} %key_w_hbm.1, bf16[2048,1024]{1,0:T(8,128)(2,1)} %value_w_hbm.1, ...), custom_call_target="tpu_custom_call" | custom-call | tf_op jit(solution)/shard_map/pallas_call | solution.py:286
  109.6 1.3 %copy.12 = bf16[1,4096,256]{2,1,0:T(8,128)(2,1)} copy(bf16[1,4096,256]{2,1,0:T(8,128)(2,1)S(1)} %bitcast.3) | data formatting | bytes 4194304
  110.9 1.3 %copy.13 = bf16[1,4096,256]{2,1,0:T(8,128)(2,1)} copy(bf16[1,4096,256]{2,1,0:T(8,128)(2,1)S(1)} %bitcast.2) | data formatting | bytes 4194304
  112.2 0.6 copy.14
Async XLA Ops:
  0.6 0.7 copy-start
  1.3 0.7 copy-start.1
  2.0 0.7 copy-start.2
